TPU v7x, 512 devices: a whole 4x8x8 slice. The times are simulated.
512 devices in a mesh: sp: 32 (over z, x), tp: 16 (over y, core).
Axes of the slice: x: 4, y: 8, z: 8, core: 2. Of those that a mesh axis runs over, the one named last changes fastest.
Arguments:
- resid: bfloat16 [4096, 2048], P('sp'), may hold values from -6 to 6
- norm_gain: float32 [2048], replicated, may hold values from 0.1 to 1.9
- cotangent: bfloat16 [4096, 2048], P('sp'), may hold values from -6 to 6
- route_ids: int32 [4096, 2], P('sp'), may hold values from 0 to 31, all different within a row; in each aligned block of 128 rows (0 to 127, 128 to 255, ...) at most 12 rows name the same one
- route_weight: float32 [4096, 2], P('sp'), may hold values from 0.25 to 2.25
- expert_gate: bfloat16 [32, 2048, 2048], P('sp', None, 'tp'), may hold values from -0.125 to 0.125
- expert_up: bfloat16 [32, 2048, 2048], P('sp', None, 'tp'), may hold values from -0.125 to 0.125
- expert_down: bfloat16 [32, 2048, 2048], P('sp', 'tp'), may hold values from -0.125 to 0.125
- out_proj: bfloat16 [2048, 4096], P('sp', 'tp'), may hold values from -0.09375 to 0.09375
- mixed: bfloat16 [4096, 4096], P('sp', 'tp'), may hold values from -6 to 6
- query: bfloat16 [4096, 2048], P('sp', 'tp'), may hold values from -6 to 6
- key: bfloat16 [4096, 2048], P('sp', 'tp'), may hold values from -1.5 to 1.5
- value: bfloat16 [4096, 4096], P('sp', 'tp'), may hold values from -6 to 6
- log_decay: float32 [4096, 2048], P('sp', 'tp'), may hold values from -1 to 0, as said below
- span_state: float32 [32, 16, 128, 256], P('sp', 'tp'), may hold values from -24 to 24
Outputs:
- grad_expert_gate: bfloat16 [32, 2048, 2048], P('sp', None, 'tp')
- grad_expert_up: bfloat16 [32, 2048, 2048], P('sp', None, 'tp')
- grad_expert_down: bfloat16 [32, 2048, 2048], P('sp', 'tp')
- grad_out_proj: float32 [2048, 4096], P('sp', 'tp')
- grad_query: bfloat16 [4096, 2048], P('sp', 'tp')
- grad_key: bfloat16 [4096, 2048], P('sp', 'tp')
- grad_value: bfloat16 [4096, 4096], P('sp', 'tp')
- grad_log_decay: float32 [4096, 2048], P('sp', 'tp')
Inputs may be any that keep to these rules, and one draw needn't show every extreme that they name: `route_ids`: A row names 2 different experts. Within each aligned block of 128 rows (the rows of one index of sp) no expert is named by more than 12 rows, and in every draw some expert is named by exactly 12 rows of some block. `log_decay`: every entry is zero or negative.
All inputs are finite; a program needn't handle non-finite values.
Results may differ from a plain program's by a relative error of at most 0.023.
Values may be sent and summed in bfloat16 or wider, within the bound.
No kernel may reach another device: no remote copies, remote signals or barrier semaphores. Data moves between devices by JAX's collectives and lax.ppermute only.
A program may use at most 64 MiB of HBM per device.

v0:
```python
import jax
import jax.numpy as jnp
from jax import lax
from jax.sharding import Mesh
from jax.sharding import PartitionSpec as P

KEY_CHANNELS = 128
DV = 256
TOP = 2
BLOCK = 64
SP = ("z", "x")
TP = ("y", "c")
epsilon = 1e-06


def sum_parts(tiles):
    return jnp.sum(tiles.astype(jnp.float32), axis=0)


def later_sum(states, decays, place):
    count = states.shape[0]
    total = jnp.zeros(states.shape[1:], jnp.float32)
    factor = jnp.ones(decays.shape[1:], jnp.float32)
    for k in range(count):
        later = k > place
        total = total + jnp.where(later, factor, 0.0)[:, None] * states[k].astype(jnp.float32)
        factor = jnp.where(later, factor * decays[k], factor)
    return (total, factor)


def to_all(array, axis):
    count = lax.axis_size(axis)
    copies = jnp.broadcast_to(array[None], (count, *array.shape))
    return lax.all_to_all(copies, axis, 0, 0, tiled=True)


def with_decay(state, decay):
    row = jnp.pad(decay[None, :], ((0, 7), (0, DV - KEY_CHANNELS)))
    return jnp.concatenate([state, row], axis=0).astype(jnp.bfloat16)


def split_decay(filled):
    decays = filled[:, KEY_CHANNELS, :KEY_CHANNELS].astype(jnp.float32)
    return (filled[:, :KEY_CHANNELS], decays)


def into_blocks(values):
    return values.reshape(values.shape[0] // BLOCK, BLOCK, values.shape[1])


def span_forward(query_rows, key_rows, value_rows, grad_rows, decay_rows, entry_state):
    query_blk = into_blocks(query_rows)
    key_blk = into_blocks(key_rows)
    value_blk = into_blocks(value_rows)
    grad_blk = into_blocks(grad_rows)
    cumlog = jnp.cumsum(into_blocks(decay_rows), axis=1)
    block_total = cumlog[:, -1, :]
    to_end = jnp.exp(block_total[:, None, :] - cumlog)
    inner_part = jnp.einsum("nsd,nsj->ndj", key_blk * to_end, value_blk)

    def forward_step(carry_state, step_item):
        piece_part, block_sum = step_item
        return (jnp.exp(block_sum)[:, None] * carry_state + piece_part, carry_state)

    end_state, starts = lax.scan(forward_step, entry_state, (inner_part, block_total))
    own_part = jnp.einsum("ntd,ntj->ndj", query_blk * jnp.exp(cumlog), grad_blk)

    def backward_step(carry_state, step_item):
        piece_part, block_sum = step_item
        return (jnp.exp(block_sum)[:, None] * carry_state + piece_part, carry_state)

    start_cot, after_cot = lax.scan(
        backward_step, jnp.zeros_like(entry_state), (own_part, block_total), reverse=True
    )
    span_total = jnp.sum(block_total, axis=0)
    later_log = span_total[None, :] - jnp.cumsum(block_total, axis=0)
    return ((cumlog, starts, after_cot, later_log, end_state), (jnp.exp(span_total), start_cot))


def span_backward(query_rows, key_rows, value_rows, grad_rows, kept_terms, exit_cot):
    cumlog, starts, after_cot, later_log, end_state = kept_terms
    query_blk = into_blocks(query_rows)
    key_blk = into_blocks(key_rows)
    value_blk = into_blocks(value_rows)
    grad_blk = into_blocks(grad_rows)
    exit_cots = after_cot + jnp.exp(later_log)[:, :, None] * exit_cot
    causal = jnp.arange(BLOCK)[:, None] >= jnp.arange(BLOCK)[None, :]
    decays = jnp.exp(
        jnp.where(causal[None, :, :, None], cumlog[:, :, None, :] - cumlog[:, None, :, :], -jnp.inf)
    )
    scores = jnp.einsum("ntd,nsd,ntsd->nts", query_blk, key_blk, decays)
    grad_scores = jnp.einsum("ntj,nsj->nts", grad_blk, value_blk)
    grad_query = jnp.exp(cumlog) * jnp.einsum("ntj,ndj->ntd", grad_blk, starts)
    grad_query = grad_query + jnp.einsum("nts,nsd,ntsd->ntd", grad_scores, key_blk, decays)
    to_end = jnp.exp(cumlog[:, -1:, :] - cumlog)
    grad_key = jnp.einsum("nts,ntd,ntsd->nsd", grad_scores, query_blk, decays)
    grad_key = grad_key + to_end * jnp.einsum("nsj,ndj->nsd", value_blk, exit_cots)
    grad_value = jnp.einsum("nts,ntj->nsj", scores, grad_blk)
    grad_value = grad_value + jnp.einsum("nsd,ndj->nsj", key_blk * to_end, exit_cots)
    length = query_rows.shape[0]
    key_width = query_rows.shape[1]
    per_position = (query_blk * grad_query - key_blk * grad_key).reshape(length, key_width)
    grad_log = (
        jnp.flip(jnp.cumsum(jnp.flip(per_position, 0), 0), 0)
        + jnp.sum(end_state * exit_cot, axis=1)[None, :]
    )
    return (
        grad_query.reshape(length, key_width),
        grad_key.reshape(length, key_width),
        grad_value.reshape(length, value_rows.shape[1]),
        grad_log,
    )


def on_device(
    resid,
    norm_gain,
    cotangent,
    route_ids,
    route_weight,
    expert_gate,
    expert_up,
    expert_down,
    out_proj,
    mixed,
    query,
    key,
    value,
    log_decay,
    span_state,
):
    tokens_here = resid.shape[0]
    model_width = resid.shape[1]
    half = model_width // 2
    sp_count = lax.axis_size(SP)
    y_count = lax.axis_size("y")
    experts = sp_count * expert_gate.shape[0]
    capacity = 3 * tokens_here // experts
    slots = experts * capacity
    core = lax.axis_index("c")
    resid_f = resid.astype(jnp.float32)
    inverse_rms = lax.rsqrt(jnp.mean(resid_f * resid_f, axis=1, keepdims=True) + epsilon)
    unit_rows = resid_f * inverse_rms
    normed = (unit_rows * norm_gain).astype(jnp.bfloat16)
    pair_expert = route_ids.reshape(-1)
    onehot = (pair_expert[:, None] == jnp.arange(experts, dtype=jnp.int32)[None, :]).astype(
        jnp.int32
    )
    slot_rank = jnp.sum((jnp.cumsum(onehot, axis=0) - onehot) * onehot, axis=1)
    slot_of = (pair_expert * capacity + slot_rank).reshape(tokens_here, TOP)
    slot_a, slot_b = (slot_of[:, 0], slot_of[:, 1])
    packed = lax.broadcasted_iota(jnp.int32, (2 * slots, 2 * tokens_here), 0)
    aim_a = jnp.concatenate([2 * slot_a, 2 * slot_a + 1])[None, :]
    aim_b = jnp.concatenate([2 * slot_b, 2 * slot_b + 1])[None, :]
    hit_a, hit_b = (packed == aim_a, packed == aim_b)
    weight_a = jnp.concatenate([route_weight[:, 0]] * 2)[None, :]
    weight_b = jnp.concatenate([route_weight[:, 1]] * 2)[None, :]
    slot_weight = jnp.sum(
        jnp.where(hit_a, weight_a, 0.0) + jnp.where(hit_b, weight_b, 0.0), axis=1, keepdims=True
    )
    scale = jnp.where(core == 0, 1.0, slot_weight)
    chosen = jnp.where(core == 0, normed, cotangent)
    rows_two = jnp.concatenate([chosen[:, :half], chosen[:, half:]], axis=0)
    sent = jnp.dot(
        (hit_a | hit_b).astype(jnp.bfloat16), rows_two, preferred_element_type=jnp.float32
    )
    sent = (sent * scale).astype(jnp.bfloat16).reshape(sp_count, 2 * capacity, half)
    own = lax.all_to_all(sent, SP, 0, 0, tiled=True).reshape(2 * slots, half)
    other = lax.ppermute(own, "c", [(0, 1), (1, 0)])
    rows_in = jnp.where(core == 0, own, other)
    rows_cot = jnp.where(core == 0, other, own)
    gate_w, up_w, down_w = (expert_gate[0], expert_up[0], expert_down[0])
    width = gate_w.shape[1]
    into_w = jnp.concatenate([gate_w[:half], gate_w[half:], up_w[:half], up_w[half:]], axis=1)
    down_two = jnp.concatenate([down_w[:, :half], down_w[:, half:]], axis=0)
    pre = jnp.dot(rows_in, into_w, preferred_element_type=jnp.float32)
    gate_pre = pre[:, :width] + jnp.roll(pre[:, width : 2 * width], -1, axis=0)
    up_pre = pre[:, 2 * width : 3 * width] + jnp.roll(pre[:, 3 * width :], -1, axis=0)
    hid = lax.dot_general(
        rows_cot, down_two, (((1,), (1,)), ((), ())), preferred_element_type=jnp.float32
    )
    grad_hidden = hid[:, :width] + jnp.roll(hid[:, width:], -1, axis=0)
    gate_sig = jax.nn.sigmoid(gate_pre)
    first = lax.broadcasted_iota(jnp.int32, (2 * slots, 1), 0) % 2 == 0

    def kept(values):
        return jnp.where(first, values, 0.0).astype(jnp.bfloat16)

    hidden = kept(gate_pre * gate_sig * up_pre)
    grad_up_act = kept(grad_hidden * gate_pre * gate_sig)
    grad_gate_act = kept(grad_hidden * up_pre * gate_sig * (1.0 + gate_pre * (1.0 - gate_sig)))
    acts = jnp.concatenate([grad_gate_act, grad_up_act], axis=1)
    pick = (
        lax.broadcasted_iota(jnp.int32, (slots, 2 * slots), 1)
        == 2 * lax.broadcasted_iota(jnp.int32, (slots, 2 * slots), 0)
    ).astype(jnp.bfloat16)
    acts = jnp.dot(pick, acts, preferred_element_type=jnp.float32).astype(jnp.bfloat16)
    out_w = jnp.concatenate([gate_w, up_w], axis=1).reshape(y_count, 2, width, 2 * width)
    out_own = jnp.where(core == 0, out_w[:, 0], out_w[:, 1]).reshape(half, 2 * width)
    out_other = jnp.where(core == 0, out_w[:, 1], out_w[:, 0]).reshape(half, 2 * width)

    def onto(weights):
        return lax.dot_general(
            acts, weights, (((1,), (1,)), ((), ())), preferred_element_type=jnp.float32
        )

    passed = lax.ppermute(onto(out_other).astype(jnp.bfloat16), "c", [(0, 1), (1, 0)])
    pair_sum = (onto(out_own) + passed.astype(jnp.float32)).astype(jnp.bfloat16)
    parts = pair_sum.reshape(slots, y_count, width).transpose(1, 0, 2)
    summed = sum_parts(lax.all_to_all(parts, "y", 0, 0, tiled=True)).astype(jnp.bfloat16)

    def beside(values):
        return jnp.concatenate([values, jnp.roll(values, 1, axis=0)], axis=1)

    grad_in_w = lax.dot_general(
        rows_in,
        jnp.concatenate([beside(grad_gate_act), beside(grad_up_act)], axis=1),
        (((0,), (0,)), ((), ())),
        preferred_element_type=jnp.float32,
    ).astype(jnp.bfloat16)
    grad_gate_w = jnp.concatenate([grad_in_w[:, :width], grad_in_w[:, width : 2 * width]], axis=0)
    grad_up_w = jnp.concatenate(
        [grad_in_w[:, 2 * width : 3 * width], grad_in_w[:, 3 * width :]], axis=0
    )
    grad_out_w = lax.dot_general(
        beside(hidden), rows_cot, (((0,), (0,)), ((), ())), preferred_element_type=jnp.float32
    ).astype(jnp.bfloat16)
    grad_down_w = jnp.concatenate([grad_out_w[:width], grad_out_w[width:]], axis=1)
    out_proj_here, own_tied = lax.optimization_barrier((out_proj, rows_in))
    out_proj_all = to_all(out_proj_here, SP).reshape(model_width, -1)
    returned = lax.all_to_all(
        summed.reshape(experts, capacity, -1), SP, split_axis=0, concat_axis=0, tiled=True
    )
    flat_rows = returned.reshape(slots, -1)
    slot_index = lax.broadcasted_iota(jnp.int32, (slots, tokens_here), 0)
    slot_tokens = ((slot_index == slot_a[None, :]) | (slot_index == slot_b[None, :])).astype(
        jnp.bfloat16
    )
    grad_normed = lax.all_gather(
        lax.dot_general(
            slot_tokens, flat_rows, (((0,), (0,)), ((), ())), preferred_element_type=jnp.float32
        ).astype(jnp.bfloat16),
        ("y", "c"),
        axis=1,
        tiled=True,
    ).astype(jnp.float32)
    scaled = grad_normed * norm_gain
    grad_resid = cotangent.astype(jnp.float32) + inverse_rms * (
        scaled - unit_rows * jnp.mean(scaled * unit_rows, axis=1, keepdims=True)
    )
    grad_resid = grad_resid.astype(jnp.bfloat16)
    grad_mixed = jnp.dot(grad_resid, out_proj_all, preferred_element_type=jnp.float32).astype(
        jnp.bfloat16
    )
    share = lax.dot_general(
        grad_resid, mixed, (((0,), (0,)), ((), ())), preferred_element_type=jnp.float32
    ).astype(jnp.bfloat16)
    grad_out_proj = sum_parts(
        lax.all_to_all(share.reshape(sp_count, model_width // sp_count, -1), SP, 0, 0, tiled=True)
    )
    head_count = query.shape[1] // KEY_CHANNELS
    query_scale = KEY_CHANNELS ** (-0.5)

    def heads_first(values, head_depth):
        return values.reshape(tokens_here, head_count, head_depth).transpose(1, 0, 2)

    query_rows = heads_first(query, KEY_CHANNELS).astype(jnp.float32) * query_scale
    key_rows = heads_first(key, KEY_CHANNELS).astype(jnp.float32)
    value_rows = heads_first(value, DV).astype(jnp.float32)
    grad_rows = heads_first(grad_mixed, DV).astype(jnp.float32)
    decay_rows = heads_first(log_decay, KEY_CHANNELS)
    kept_terms, summary = jax.vmap(span_forward)(
        query_rows, key_rows, value_rows, grad_rows, decay_rows, span_state[0]
    )
    own_decay, own_state = (summary[0][0], summary[1][0])
    near_states, near_decays = split_decay(to_all(with_decay(own_state, own_decay), "x"))
    near_sum, near_factor = later_sum(near_states, near_decays, lax.axis_index("x"))
    group_sum, group_factor = later_sum(near_states, near_decays, -1)
    far_states, far_decays = split_decay(to_all(with_decay(group_sum, group_factor), "z"))
    far_sum, _ = later_sum(far_states, far_decays, lax.axis_index("z"))
    exit_cot = near_sum + near_factor[:, None] * far_sum
    head_grads = jax.vmap(span_backward)(
        query_rows, key_rows, value_rows, grad_rows, kept_terms, exit_cot[None]
    )

    def tokens_first(values):
        return values.transpose(1, 0, 2).reshape(tokens_here, -1)

    grad_query = (tokens_first(head_grads[0]) * query_scale).astype(jnp.bfloat16)
    grad_key = tokens_first(head_grads[1]).astype(jnp.bfloat16)
    grad_value = tokens_first(head_grads[2]).astype(jnp.bfloat16)
    grad_log_decay = tokens_first(head_grads[3])
    return (
        grad_gate_w[None],
        grad_up_w[None],
        grad_down_w[None],
        grad_out_proj,
        grad_query,
        grad_key,
        grad_value,
        grad_log_decay,
    )


def solution(mesh):
    finer = Mesh(mesh.devices.reshape(8, 4, 8, 2), ("z", "x", "y", "c"))
    in_specs = (
        P(SP, None),
        P(),
        P(SP, None),
        P(SP, None),
        P(SP, None),
        P(SP, None, TP),
        P(SP, None, TP),
        P(SP, TP, None),
        P(SP, TP),
        P(SP, TP),
        P(SP, TP),
        P(SP, TP),
        P(SP, TP),
        P(SP, TP),
        P(SP, TP, None, None),
    )
    out_specs = (
        P(SP, None, TP),
        P(SP, None, TP),
        P(SP, TP, None),
        P(SP, TP),
        P(SP, TP),
        P(SP, TP),
        P(SP, TP),
        P(SP, TP),
    )
    return jax.shard_map(
        on_device, mesh=finer, in_specs=in_specs, out_specs=out_specs, check_vma=False
    )
```

profile of v0, /device:TPU:2, one launch (start us, length us, event | category | flops | bytes accessed | tf_op | source)
XLA Modules:
  0.0 222.4 jit_solution(10590077181551964781)
XLA Ops:
  0.7 0.9 copy.91
  1.8 0.8 slice_bitcast_fusion.11
  2.6 0.6 reduce-window.6
  3.7 0.7 multiply_add_fusion
  4.5 1.2 fusion.22
  6.2 1.0 fusion.48
  7.2 1.8 multiply_convert_fusion
  9.0 13.6 %all-to-all-start = ((bf16[32,24,1024]{2,1,0:T(8,128)(2,1)}), bf16[32,24,1024]{2,1,0:T(8,128)(2,1)S(1)}, u32[]{:S(2)}, u32[]{:S(2)}) async-start(bf16[32,24,1024]{2,1,0:T(8,128)(2,1)} %bitcast.383), calls=%async_computation | async-start | bytes 3145728 | tf_op jit(solution)/shard_map/all_to_all | solution.py:168
  22.7 0.6 iota_multiply_fusion
  23.3 0.7 broadcast_convert_fusion
  24.0 0.6 slice_reduce_fusion.1
  24.8 0.5 convert_bitcast_fusion.13
  25.3 35.7 %all-to-all-done = bf16[32,24,1024]{2,1,0:T(8,128)(2,1)S(1)} async-done(((bf16[32,24,1024]{2,1,0:T(8,128)(2,1)}), bf16[32,24,1024]{2,1,0:T(8,128)(2,1)S(1)}, u32[]{:S(2)}, u32[]{:S(2)}) %all-to-all-start) | async-done | bytes 1572896 | tf_op jit(solution)/shard_map/all_to_all | solution.py:168
  61.0 1.9 collective-permute-start
  63.0 2.3 %broadcast_select_fusion.4 = (bf16[8,1,128,256]{3,2,1,0:T(8,128)(2,1)S(1)}, bf16[8,1,128,256]{3,2,1,0:T(8,128)(2,1)}) fusion(pred[]{:T(512)S(6)} %eq.83, bf16[8,2,128,128]{3,2,1,0:T(8,128)(2,1)S(1)} %bitcast.376, bf16[8,2,128,128]{3,2,1,0:T(8,128)(2,1)} %bitcast.377), kind=kLoop, calls=%fused_computation.94 | loop fusion | flops 3670016 | bytes 2097153 | tf_op jit(solution)/shard_map/jit(_where)/select_n | solution.py:200
  65.2 0.6 slice_bitcast_fusion.13
  65.9 0.7 convert_bitcast_fusion.11
  67.0 1.0 fusion.23
  68.2 2.0 fusion.45
  70.3 0.9 select_convert_fusion
  71.5 0.3 copy-done.35
  71.8 0.4 fusion.11
  72.2 1.3 convolution_convert_fusion.2
  73.5 2.3 %collective-permute-start.1 = (bf16[384,1024]{1,0:T(8,128)(2,1)}, bf16[384,1024]{1,0:T(8,128)(2,1)}, u32[]{:S(2)}, u32[]{:S(2)}) collective-permute-start(bf16[384,1024]{1,0:T(8,128)(2,1)} %convolution_convert_fusion.2), channel_id=1, source_target_pairs={{0,1},{1,0},{2,3},{3,2},{4,5},{5,4},{6,7},{7,6},{8,9},{9,8},{10,11... | collective-permute-start | bytes 2359304 | tf_op jit(solution)/shard_map/ppermute | solution.py:207
  75.8 1.5 while.29
  75.9 0.6 bitcast_dynamic-update-slice_fusion.4
  76.6 0.6 bitcast_dynamic-update-slice_fusion.4
  77.4 0.6 collective-permute-done.1
  78.0 1.5 fusion.31
  79.6 1.1 copy.125
  80.7 7.1 %all-to-all-start.1 = ((bf16[8,384,128]{2,1,0:T(8,128)(2,1)}), bf16[8,384,128]{2,1,0:T(8,128)(2,1)S(1)}, u32[]{:S(2)}, u32[]{:S(2)}) async-start(bf16[8,384,128]{2,1,0:T(8,128)(2,1)} %bitcast.374), calls=%async_computation.1 | async-start | bytes 1572864 | tf_op jit(solution)/shard_map/all_to_all | solution.py:210
  87.9 4.4 %fusion.4 = (bf16[2,64,64]{2,1,0:T(8,128)(2,1)}, f32[2,64,128,64]{2,3,1,0:T(8,128)}) fusion(f32[2,128,64]{1,2,0:T(8,128)S(1)} %copy-done.21, f32[2,128,64]{1,2,0:T(8,128)S(1)} %bitcast.384, f32[2,64,128]{2,1,0:T(8,128)S(1)} %bitcast.371, pred[64,64]{1,0:T(8,128)(4,1)S(1)} %iota_compare_fusion.10), kind=kLoop, calls=%fused_computation.11 | loop fusion | flops 5234688 | bytes 4411392 | tf_op jit(solution)/shard_map/vmap(ntd,nsd,ntsd->nts)/dot_general | solution.py:91
  92.3 1.0 convolution_convert_fusion.1
  93.3 1.0 fusion.147
  94.3 2.8 %convolution_convert_fusion.3 = bf16[256,1024]{1,0:T(8,128)(2,1)} fusion(bf16[768,1024]{1,0:T(8,128)(2,1)} %collective-permute-done, bf16[768,1024]{1,0:T(8,128)(2,1)S(1)} %bitcast.370, pred[]{:T(512)S(6)} %eq.83, bf16[767,128]{1,0:T(8,128)(2,1)S(1)} %bitcast.395, bf16[1,128]{1,0:T(2,128)(2,1)S(1)} %slice.339, bf16[768,128]{1,0:T(8,128)(2,1)S(1)} %copy-done.22), kind=kOutput, calls=%fused_computation.30 | convolution fusion | flops 404881408 | bytes 4063233 | tf_op jit(solution)/shard_map/dot_general | solution.py:225
  97.1 14.4 %all-to-all-done.1 = bf16[8,384,128]{2,1,0:T(8,128)(2,1)S(1)} async-done(((bf16[8,384,128]{2,1,0:T(8,128)(2,1)}), bf16[8,384,128]{2,1,0:T(8,128)(2,1)S(1)}, u32[]{:S(2)}, u32[]{:S(2)}) %all-to-all-start.1) | async-done | bytes 786464 | tf_op jit(solution)/shard_map/all_to_all | solution.py:210
  111.6 0.7 reshape.961
  112.3 6.5 %all-to-all-start.2 = ((bf16[32,12,128]{2,1,0:T(8,128)(2,1)}), bf16[32,12,128]{2,1,0:T(8,128)(2,1)S(1)}, u32[]{:S(2)}, u32[]{:S(2)}) async-start(bf16[32,12,128]{2,1,0:T(8,128)(2,1)} %reshape.961), calls=%async_computation.2 | async-start | bytes 262144 | tf_op jit(solution)/shard_map/all_to_all | solution.py:231
  118.8 1.9 maximum_bitcast_fusion
  120.7 7.1 %all-to-all-done.2 = bf16[32,12,128]{2,1,0:T(8,128)(2,1)S(1)} async-done(((bf16[32,12,128]{2,1,0:T(8,128)(2,1)}), bf16[32,12,128]{2,1,0:T(8,128)(2,1)S(1)}, u32[]{:S(2)}, u32[]{:S(2)}) %all-to-all-start.2) | async-done | bytes 98336 | tf_op jit(solution)/shard_map/all_to_all | solution.py:231
  127.8 1.2 broadcast_in_dim.169
  129.0 5.6 %all-to-all-start.4 = ((bf16[32,64,256]{2,1,0:T(8,128)(2,1)}), bf16[32,64,256]{2,1,0:T(8,128)(2,1)S(1)}, u32[]{:S(2)}, u32[]{:S(2)}) async-start(bf16[32,64,256]{2,1,0:T(8,128)(2,1)} %broadcast_in_dim.169), calls=%async_computation.4 | async-start | bytes 2097152 | tf_op jit(solution)/shard_map/all_to_all | solution.py:34
  134.6 0.8 maximum_bitcast_fusion.1
  135.5 0.8 maximum_bitcast_fusion.2
  136.7 16.1 %all_gather.3 = bf16[128,2048]{1,0:T(8,128)(2,1)S(1)} all-gather(bf16[128,128]{1,0:T(8,128)(2,1)S(1)} %convolution_convert_fusion.5), channel_id=1, replica_groups=mesh['z'=8,'x'=4,'y'=8,'c'=2] {'y','c'}, dimensions={1}, use_global_device_ids=true | all-gather | bytes 557056 | tf_op jit(solution)/shard_map/all_gather | solution.py:239
  153.1 0.4 fusion.21
  153.6 8.0 %all-to-all-done.4 = bf16[32,64,256]{2,1,0:T(8,128)(2,1)S(1)} async-done(((bf16[32,64,256]{2,1,0:T(8,128)(2,1)}), bf16[32,64,256]{2,1,0:T(8,128)(2,1)S(1)}, u32[]{:S(2)}, u32[]{:S(2)}) %all-to-all-start.4) | async-done | bytes 1048608 | tf_op jit(solution)/shard_map/all_to_all | solution.py:34
  162.2 0.3 while.30
  162.8 0.7 broadcast_in_dim.173
  163.5 4.9 %all-to-all-start.5 = ((bf16[4,136,256]{2,1,0:T(8,128)(2,1)}), bf16[4,136,256]{2,1,0:T(8,128)(2,1)S(1)}, u32[]{:S(2)}, u32[]{:S(2)}) async-start(bf16[4,136,256]{2,1,0:T(8,128)(2,1)} %broadcast_in_dim.173), calls=%async_computation.5 | async-start | bytes 557056 | tf_op jit(solution)/shard_map/all_to_all | solution.py:34
  168.7 5.1 %all-to-all-done.5 = bf16[4,136,256]{2,1,0:T(8,128)(2,1)S(1)} async-done(((bf16[4,136,256]{2,1,0:T(8,128)(2,1)}), bf16[4,136,256]{2,1,0:T(8,128)(2,1)S(1)}, u32[]{:S(2)}, u32[]{:S(2)}) %all-to-all-start.5) | async-done | bytes 278560 | tf_op jit(solution)/shard_map/all_to_all | solution.py:34
  174.0 0.9 broadcast_in_dim.175
  174.8 3.5 %all-to-all-start.6 = ((bf16[8,136,256]{2,1,0:T(8,128)(2,1)}), bf16[8,136,256]{2,1,0:T(8,128)(2,1)S(1)}, u32[]{:S(2)}, u32[]{:S(2)}) async-start(bf16[8,136,256]{2,1,0:T(8,128)(2,1)} %broadcast_in_dim.175), calls=%async_computation.6 | async-start | bytes 1114112 | tf_op jit(solution)/shard_map/all_to_all | solution.py:34
  178.4 5.0 %fusion.5 = f32[2,64,128]{2,1,0:T(8,128)S(1)} fusion(f32[2,64,128,64]{2,3,1,0:T(8,128)} %get-tuple-element.289, f32[2,64,128]{2,1,0:T(8,128)S(1)} %copy-done.20, f32[2,64,64]{2,1,0:T(8,128)S(1)} %copy.98), kind=kLoop, calls=%fused_computation.13 | loop fusion | flops 3129344 | bytes 4358144 | tf_op jit(solution)/shard_map/vmap(nts,nsd,ntsd->ntd)/dot_general | solution.py:94
  183.6 1.4 convolution_convert_fusion
  185.0 2.0 multiply_reduce_fusion
  187.0 6.0 %all-to-all-done.6 = bf16[8,136,256]{2,1,0:T(8,128)(2,1)S(1)} async-done(((bf16[8,136,256]{2,1,0:T(8,128)(2,1)}), bf16[8,136,256]{2,1,0:T(8,128)(2,1)S(1)}, u32[]{:S(2)}, u32[]{:S(2)}) %all-to-all-start.6) | async-done | bytes 557088 | tf_op jit(solution)/shard_map/all_to_all | solution.py:34
  193.0 5.0 %all-to-all-start.3 = ((bf16[32,64,256]{2,1,0:T(8,128)(2,1)}), bf16[32,64,256]{2,1,0:T(8,128)(2,1)S(1)}, u32[]{:S(2)}, u32[]{:S(2)}) async-start(bf16[32,64,256]{2,1,0:T(8,128)(2,1)} %bitcast.28), calls=%async_computation.3 | async-start | bytes 2097152 | tf_op jit(solution)/shard_map/all_to_all | solution.py:259
  198.4 0.9 multiply_subtract_fusion
  199.5 0.3 fusion.81
  199.8 0.6 add_bitcast_fusion
  200.7 0.8 fusion.12
  201.6 20.1 %all-to-all-done.3 = bf16[32,64,256]{2,1,0:T(8,128)(2,1)S(1)} async-done(((bf16[32,64,256]{2,1,0:T(8,128)(2,1)}), bf16[32,64,256]{2,1,0:T(8,128)(2,1)S(1)}, u32[]{:S(2)}, u32[]{:S(2)}) %all-to-all-start.3) | async-done | bytes 1048608 | tf_op jit(solution)/shard_map/all_to_all | solution.py:259
  221.6 0.8 convert_reduce_fusion
  (157 shorter events, 6.1 us)
Async XLA Ops:
  0.6 182.9 %copy-start = (bf16[128,256]{1,0:T(8,128)(2,1)S(1)}, bf16[128,256]{1,0:T(8,128)(2,1)}, u32[]{:S(2)}) copy-start(bf16[128,256]{1,0:T(8,128)(2,1)} %param.28) | copy-start | bytes 196612
  0.6 5.5 %copy-start.2 = (bf16[128,2048]{1,0:T(8,128)(2,1)S(1)}, bf16[128,2048]{1,0:T(8,128)(2,1)}, u32[]{:S(2)}) copy-start(bf16[128,2048]{1,0:T(8,128)(2,1)} %param.19) | copy-start | bytes 1572868
  0.7 5.5 %copy-start.6 = (bf16[128,2048]{1,0:T(8,128)(2,1)S(1)}, bf16[128,2048]{1,0:T(8,128)(2,1)}, u32[]{:S(2)}) copy-start(bf16[128,2048]{1,0:T(8,128)(2,1)} %param.21) | copy-start | bytes 1572868
  5.7 0.5 copy-start.33
  9.0 13.6 %copy-start.31 = (f32[128,128]{1,0:T(8,128)S(1)}, f32[128,128]{1,0:T(8,128)}, u32[]{:S(2)}) copy-start(f32[128,128]{1,0:T(8,128)} %param.32) | copy-start | bytes 196612
  9.0 15.6 %copy-start.13 = (bf16[128,256]{1,0:T(8,128)(2,1)S(1)}, bf16[128,256]{1,0:T(8,128)(2,1)}, u32[]{:S(2)}) copy-start(bf16[128,256]{1,0:T(8,128)(2,1)} %param.31) | copy-start | bytes 196612
  9.0 15.6 %copy-start.18 = (bf16[128,128]{1,0:T(8,128)(2,1)S(1)}, bf16[128,128]{1,0:T(8,128)(2,1)}, u32[]{:S(2)}) copy-start(bf16[128,128]{1,0:T(8,128)(2,1)} %param.30) | copy-start | bytes 98308
  9.0 54.0 %copy-start.3 = (bf16[1,2048,128]{2,1,0:T(8,128)(2,1)S(1)}, bf16[1,2048,128]{2,1,0:T(8,128)(2,1)}, u32[]{:S(2)}) copy-start(bf16[1,2048,128]{2,1,0:T(8,128)(2,1)} %param.25) | copy-start | bytes 1572868
  9.0 52.0 %all-to-all-start = ((bf16[32,24,1024]{2,1,0:T(8,128)(2,1)}), bf16[32,24,1024]{2,1,0:T(8,128)(2,1)S(1)}, u32[]{:S(2)}, u32[]{:S(2)}) async-start(bf16[32,24,1024]{2,1,0:T(8,128)(2,1)} %bitcast.383), calls=%async_computation | async-start | bytes 3145728 | tf_op jit(solution)/shard_map/all_to_all | solution.py:168
  22.6 43.2 %copy-start.28 = (bf16[128,128]{1,0:T(8,128)(2,1)S(1)}, bf16[128,128]{1,0:T(8,128)(2,1)}, u32[]{:S(2)}) copy-start(bf16[128,128]{1,0:T(8,128)(2,1)} %param.29) | copy-start | bytes 98308
  61.0 5.7 %collective-permute-start = (bf16[768,1024]{1,0:T(8,128)(2,1)S(1)}, bf16[768,1024]{1,0:T(8,128)(2,1)}, u32[]{:S(2)}, u32[]{:S(2)}) collective-permute-start(bf16[768,1024]{1,0:T(8,128)(2,1)S(1)} %bitcast.368), channel_id=1, source_target_pairs={{0,1},{1,0},{2,3},{3,2},{4,5},{5,4},{6,7},{7,6},{8,9},{9,8},{10,11... | collective-permute-start | bytes 4718600 | tf_op jit(solution)/shard_map/ppermute | solution.py:169
  62.9 3.6 %copy-start.16 = (bf16[1,128,2048]{2,1,0:T(8,128)(2,1)S(1)}, bf16[1,128,2048]{2,1,0:T(8,128)(2,1)}, u32[]{:S(2)}) copy-start(bf16[1,128,2048]{2,1,0:T(8,128)(2,1)} %param.26) | copy-start | bytes 1572868
  63.0 3.6 %copy-start.4 = (bf16[1,2048,128]{2,1,0:T(8,128)(2,1)S(1)}, bf16[1,2048,128]{2,1,0:T(8,128)(2,1)}, u32[]{:S(2)}) copy-start(bf16[1,2048,128]{2,1,0:T(8,128)(2,1)} %param.24) | copy-start | bytes 1572868
  65.9 21.9 %copy-start.11 = (f32[128,128]{1,0:T(8,128)}, f32[128,128]{1,0:T(8,128)S(1)}, u32[]{:S(2)}) copy-start(f32[128,128]{1,0:T(8,128)S(1)} %convert_multiply_fusion.18) | copy-start | bytes 196612
  67.0 1.1 copy-start.8
  71.1 0.7 copy-start.35
  71.4 4.4 %copy-start.23 = (bf16[768,128]{1,0:T(8,128)(2,1)}, bf16[768,128]{1,0:T(8,128)(2,1)S(1)}, u32[]{:S(2)}) copy-start(bf16[768,128]{1,0:T(8,128)(2,1)S(1)} %get-tuple-element.266) | copy-start | bytes 589828
  71.4 4.4 %copy-start.25 = (bf16[768,128]{1,0:T(8,128)(2,1)}, bf16[768,128]{1,0:T(8,128)(2,1)S(1)}, u32[]{:S(2)}) copy-start(bf16[768,128]{1,0:T(8,128)(2,1)S(1)} %get-tuple-element.267) | copy-start | bytes 589828
  71.4 4.4 %copy-start.1 = (f32[1,1,128,256]{3,2,1,0:T(8,128)S(1)}, f32[1,1,128,256]{3,2,1,0:T(8,128)}, u32[]{:S(2)}) copy-start(f32[1,1,128,256]{3,2,1,0:T(8,128)} %param.33) | copy-start | bytes 393220
  71.5 4.4 %copy-start.36 = (f32[2,1,128]{2,1,0:T(1,128)S(1)}, f32[2,1,128]{2,1,0:T(1,128)}, u32[]{:S(2)}) copy-start(f32[2,1,128]{2,1,0:T(1,128)} %get-tuple-element.408) | copy-start | bytes 3076
  73.5 4.5 %collective-permute-start.1 = (bf16[384,1024]{1,0:T(8,128)(2,1)}, bf16[384,1024]{1,0:T(8,128)(2,1)}, u32[]{:S(2)}, u32[]{:S(2)}) collective-permute-start(bf16[384,1024]{1,0:T(8,128)(2,1)} %convolution_convert_fusion.2), channel_id=1, source_target_pairs={{0,1},{1,0},{2,3},{3,2},{4,5},{5,4},{6,7},{7,6},{8,9},{9,8},{10,11... | collective-permute-start | bytes 2359304 | tf_op jit(solution)/shard_map/ppermute | solution.py:207
  75.8 2.2 copy-start.5
  79.6 8.2 %copy-start.21 = (f32[2,128,64]{1,2,0:T(8,128)S(1)}, f32[2,128,64]{1,2,0:T(8,128)}, u32[]{:S(2)}) copy-start(f32[2,128,64]{1,2,0:T(8,128)} %get-tuple-element.296) | copy-start | bytes 196612
  80.7 30.8 %all-to-all-start.1 = ((bf16[8,384,128]{2,1,0:T(8,128)(2,1)}), bf16[8,384,128]{2,1,0:T(8,128)(2,1)S(1)}, u32[]{:S(2)}, u32[]{:S(2)}) async-start(bf16[8,384,128]{2,1,0:T(8,128)(2,1)} %bitcast.374), calls=%async_computation.1 | async-start | bytes 1572864 | tf_op jit(solution)/shard_map/all_to_all | solution.py:210
  87.8 4.4 %copy-start.26 = (bf16[768,128]{1,0:T(8,128)(2,1)S(1)}, bf16[768,128]{1,0:T(8,128)(2,1)}, u32[]{:S(2)}) copy-start(bf16[768,128]{1,0:T(8,128)(2,1)} %copy-done.25) | copy-start | bytes 589828
  87.8 4.4 %copy-start.24 = (bf16[768,128]{1,0:T(8,128)(2,1)S(1)}, bf16[768,128]{1,0:T(8,128)(2,1)}, u32[]{:S(2)}) copy-start(bf16[768,128]{1,0:T(8,128)(2,1)} %copy-done.23) | copy-start | bytes 589828
  87.8 4.4 %copy-start.22 = (bf16[768,128]{1,0:T(8,128)(2,1)S(1)}, bf16[768,128]{1,0:T(8,128)(2,1)}, u32[]{:S(2)}) copy-start(bf16[768,128]{1,0:T(8,128)(2,1)} %get-tuple-element.264) | copy-start | bytes 589828
  87.8 4.4 %copy-start.9 = (bf16[768,1024]{1,0:T(8,128)(2,1)S(1)}, bf16[768,1024]{1,0:T(8,128)(2,1)}, u32[]{:S(2)}) copy-start(bf16[768,1024]{1,0:T(8,128)(2,1)} %copy-done.8) | copy-start | bytes 4718596
  97.1 30.7 %copy-start.32 = (bf16[64,256]{1,0:T(8,128)(2,1)S(1)}, bf16[64,256]{1,0:T(8,128)(2,1)}, u32[]{:S(2)}) copy-start(bf16[64,256]{1,0:T(8,128)(2,1)} %param.27) | copy-start | bytes 98308
  112.3 15.5 %all-to-all-start.2 = ((bf16[32,12,128]{2,1,0:T(8,128)(2,1)}), bf16[32,12,128]{2,1,0:T(8,128)(2,1)S(1)}, u32[]{:S(2)}, u32[]{:S(2)}) async-start(bf16[32,12,128]{2,1,0:T(8,128)(2,1)} %reshape.961), calls=%async_computation.2 | async-start | bytes 262144 | tf_op jit(solution)/shard_map/all_to_all | solution.py:231
  120.7 13.9 %copy-start.10 = (bf16[1024,128]{1,0:T(8,128)(2,1)S(1)}, bf16[1024,128]{1,0:T(8,128)(2,1)}, u32[]{:S(2)}) copy-start(bf16[1024,128]{1,0:T(8,128)(2,1)} %get-tuple-element.275) | copy-start | bytes 786436
  129.0 6.5 %copy-start.17 = (bf16[256,1024]{1,0:T(8,128)(2,1)S(1)}, bf16[256,1024]{1,0:T(8,128)(2,1)}, u32[]{:S(2)}) copy-start(bf16[256,1024]{1,0:T(8,128)(2,1)} %convolution_convert_fusion.3) | copy-start | bytes 1572868
  129.0 32.6 %all-to-all-start.4 = ((bf16[32,64,256]{2,1,0:T(8,128)(2,1)}), bf16[32,64,256]{2,1,0:T(8,128)(2,1)S(1)}, u32[]{:S(2)}, u32[]{:S(2)}) async-start(bf16[32,64,256]{2,1,0:T(8,128)(2,1)} %broadcast_in_dim.169), calls=%async_computation.4 | async-start | bytes 2097152 | tf_op jit(solution)/shard_map/all_to_all | solution.py:34
  134.6 1.8 copy-start.39
  134.6 1.8 copy-start.40
  135.5 17.3 %copy-start.30 = (f32[2048]{0:T(1024)S(1)}, f32[2048]{0:T(1024)}, u32[]{:S(2)}) copy-start(f32[2048]{0:T(1024)} %param.20) | copy-start | bytes 24580
  135.5 17.3 %copy-start.34 = (f32[128]{0:T(128)S(1)}, f32[128]{0:T(128)}, u32[]{:S(2)}) copy-start(f32[128]{0:T(128)} %copy-done.33) | copy-start | bytes 1540
  135.5 17.6 %copy-start.7 = (bf16[128,2048]{1,0:T(8,128)(2,1)S(1)}, bf16[128,2048]{1,0:T(8,128)(2,1)}, u32[]{:S(2)}) copy-start(bf16[128,2048]{1,0:T(8,128)(2,1)} %param.21) | copy-start | bytes 1572868
  153.1 8.8 %copy-start.12 = (f32[128,128]{1,0:T(8,128)S(1)}, f32[128,128]{1,0:T(8,128)}, u32[]{:S(2)}) copy-start(f32[128,128]{1,0:T(8,128)} %copy-done.11) | copy-start | bytes 196612
  153.6 8.6 %copy-start.37 = (f32[2,1,128]{2,1,0:T(1,128)S(1)}, f32[2,1,128]{2,1,0:T(1,128)}, u32[]{:S(2)}) copy-start(f32[2,1,128]{2,1,0:T(1,128)} %get-tuple-element.408) | copy-start | bytes 3076
  162.2 0.6 copy-start.38
  162.2 6.3 %copy-start.14 = (bf16[128,256]{1,0:T(8,128)(2,1)S(1)}, bf16[128,256]{1,0:T(8,128)(2,1)}, u32[]{:S(2)}) copy-start(bf16[128,256]{1,0:T(8,128)(2,1)} %param.31) | copy-start | bytes 196612
  163.5 14.8 %copy-start.20 = (f32[2,64,128]{2,1,0:T(8,128)S(1)}, f32[2,64,128]{2,1,0:T(8,128)}, u32[]{:S(2)}) copy-start(f32[2,64,128]{2,1,0:T(8,128)} %get-tuple-element.297) | copy-start | bytes 196612
  163.5 10.2 %all-to-all-start.5 = ((bf16[4,136,256]{2,1,0:T(8,128)(2,1)}), bf16[4,136,256]{2,1,0:T(8,128)(2,1)S(1)}, u32[]{:S(2)}, u32[]{:S(2)}) async-start(bf16[4,136,256]{2,1,0:T(8,128)(2,1)} %broadcast_in_dim.173), calls=%async_computation.5 | async-start | bytes 557056 | tf_op jit(solution)/shard_map/all_to_all | solution.py:34
  174.8 18.2 %all-to-all-start.6 = ((bf16[8,136,256]{2,1,0:T(8,128)(2,1)}), bf16[8,136,256]{2,1,0:T(8,128)(2,1)S(1)}, u32[]{:S(2)}, u32[]{:S(2)}) async-start(bf16[8,136,256]{2,1,0:T(8,128)(2,1)} %broadcast_in_dim.175), calls=%async_computation.6 | async-start | bytes 1114112 | tf_op jit(solution)/shard_map/all_to_all | solution.py:34
  178.4 5.0 %copy-start.15 = (bf16[2,1,128,256]{3,2,1,0:T(8,128)(2,1)S(1)}, bf16[2,1,128,256]{3,2,1,0:T(8,128)(2,1)}, u32[]{:S(2)}) copy-start(bf16[2,1,128,256]{3,2,1,0:T(8,128)(2,1)} %get-tuple-element.142) | copy-start | bytes 393220
  187.0 11.4 %copy-start.19 = (bf16[128,128]{1,0:T(8,128)(2,1)S(1)}, bf16[128,128]{1,0:T(8,128)(2,1)}, u32[]{:S(2)}) copy-start(bf16[128,128]{1,0:T(8,128)(2,1)} %param.30) | copy-start | bytes 98308
  187.0 11.4 %copy-start.29 = (bf16[128,128]{1,0:T(8,128)(2,1)S(1)}, bf16[128,128]{1,0:T(8,128)(2,1)}, u32[]{:S(2)}) copy-start(bf16[128,128]{1,0:T(8,128)(2,1)} %param.29) | copy-start | bytes 98308
  193.0 28.6 %all-to-all-start.3 = ((bf16[32,64,256]{2,1,0:T(8,128)(2,1)}), bf16[32,64,256]{2,1,0:T(8,128)(2,1)S(1)}, u32[]{:S(2)}, u32[]{:S(2)}) async-start(bf16[32,64,256]{2,1,0:T(8,128)(2,1)} %bitcast.28), calls=%async_computation.3 | async-start | bytes 2097152 | tf_op jit(solution)/shard_map/all_to_all | solution.py:259
  198.4 2.3 %copy-start.27 = (bf16[2,64,64]{2,1,0:T(8,128)(2,1)S(1)}, bf16[2,64,64]{2,1,0:T(8,128)(2,1)}, u32[]{:S(2)}) copy-start(bf16[2,64,64]{2,1,0:T(8,128)(2,1)} %get-tuple-element.288) | copy-start | bytes 49156
where the time goes:
time: 224 us; the launch traced here: 222 us
  waiting for transfers between devices  97 us (43%)
  starting transfers between devices  50.6 us (23%)
  other arithmetic  29.2 us (13%)
  matrix products  16.6 us (7%)
  blocking collectives  16.1 us (7%)
  local copies, waits for them, and re-layouts  11.3 us (5%)
    all_to_all x1, waiting for transfers between devices, on_device(): own = lax.all_to_all(sent, SP, 0, 0, tiled=True).reshape(2 * slots, half)  35.7 us
    all_to_all x1, waiting for transfers between devices, on_device(): lax.all_to_all(share.reshape(sp_count, model_width // sp_count, -1), SP,...  20.1 us
    all_to_all x3, waiting for transfers between devices, to_all(): return lax.all_to_all(copies, axis, 0, 0, tiled=True)  19.1 us
    all_gather x1, blocking collectives, on_device(): lax.all_gather(lax.dot_general(slot_tokens, flat_rows, (((0,), (0,)), (()...  16.1 us
    all_to_all x1, waiting for transfers between devices, on_device(): lax.all_to_all(parts, 'y', 0, 0, tiled=True)  14.4 us
    all_to_all x3, starting transfers between devices, to_all(): return lax.all_to_all(copies, axis, 0, 0, tiled=True)  14.1 us
    all_to_all x1, starting transfers between devices, on_device(): own = lax.all_to_all(sent, SP, 0, 0, tiled=True).reshape(2 * slots, half)  13.6 us
    all_to_all x1, waiting for transfers between devices, on_device(): lax.all_to_all(summed.reshape(experts, capacity, -1), SP, split_axis=0, c...  7.14 us
  transfers between devices with their start and end apart: 9, of which 8 were waited for; matrix products, arithmetic and copies ran while one was open for 15% of the time, Pallas kernels for 0%

commit v1 on v0

--- a/solution.py
+++ b/solution.py
@@ -236,13 +236,14 @@
     slot_tokens = ((slot_index == slot_a[None, :]) | (slot_index == slot_b[None, :])).astype(
         jnp.bfloat16
     )
-    grad_normed = lax.all_gather(
-        lax.dot_general(
-            slot_tokens, flat_rows, (((0,), (0,)), ((), ())), preferred_element_type=jnp.float32
-        ).astype(jnp.bfloat16),
-        ("y", "c"),
+    grad_normed = jnp.concatenate(
+        lax.all_gather(
+            lax.dot_general(
+                slot_tokens, flat_rows, (((0,), (0,)), ((), ())), preferred_element_type=jnp.float32
+            ).astype(jnp.bfloat16),
+            ("y", "c"),
+        ),
         axis=1,
-        tiled=True,
     ).astype(jnp.float32)
     scaled = grad_normed * norm_gain
     grad_resid = cotangent.astype(jnp.float32) + inverse_rms * (

time: 224 us -> 224 us (level)
  no operation moved by 1% of the time
where the time goes in v1:
time: 224 us; the launch traced here: 222 us
  waiting for transfers between devices  97 us (43%)
  starting transfers between devices  50.6 us (23%)
  other arithmetic  29.2 us (13%)
  matrix products  16.6 us (7%)
  blocking collectives  16.1 us (7%)
  local copies, waits for them, and re-layouts  11.3 us (5%)
    all_to_all x1, waiting for transfers between devices, on_device(): own = lax.all_to_all(sent, SP, 0, 0, tiled=True).reshape(2 * slots, half)  35.7 us
    all_to_all x1, waiting for transfers between devices, on_device(): lax.all_to_all(share.reshape(sp_count, model_width // sp_count, -1), SP,...  20.1 us
    all_to_all x3, waiting for transfers between devices, to_all(): return lax.all_to_all(copies, axis, 0, 0, tiled=True)  19.1 us
    all_gather x1, blocking collectives, on_device(): lax.all_gather(lax.dot_general(slot_tokens, flat_rows, (((0,), (0,)), (()...  16.1 us
    all_to_all x1, waiting for transfers between devices, on_device(): lax.all_to_all(parts, 'y', 0, 0, tiled=True)  14.4 us
    all_to_all x3, starting transfers between devices, to_all(): return lax.all_to_all(copies, axis, 0, 0, tiled=True)  14.1 us
    all_to_all x1, starting transfers between devices, on_device(): own = lax.all_to_all(sent, SP, 0, 0, tiled=True).reshape(2 * slots, half)  13.6 us
    all_to_all x1, waiting for transfers between devices, on_device(): lax.all_to_all(summed.reshape(experts, capacity, -1), SP, split_axis=0, c...  7.14 us
  transfers between devices with their start and end apart: 9, of which 8 were waited for; matrix products, arithmetic and copies ran while one was open for 15% of the time, Pallas kernels for 0%

profile of v1, /device:TPU:2, one launch (start us, length us, event | category | flops | bytes accessed | tf_op | source)
XLA Modules:
  0.0 222.4 jit_solution(335717066944635824)
XLA Ops:
  0.7 0.9 copy.97
  1.8 0.8 slice_bitcast_fusion.11
  2.6 0.6 reduce-window.6
  3.7 0.7 multiply_add_fusion
  4.5 1.2 fusion.22
  6.2 1.0 fusion.48
  7.2 1.8 multiply_convert_fusion
  9.0 13.6 %all-to-all-start = ((bf16[32,24,1024]{2,1,0:T(8,128)(2,1)}), bf16[32,24,1024]{2,1,0:T(8,128)(2,1)S(1)}, u32[]{:S(2)}, u32[]{:S(2)}) async-start(bf16[32,24,1024]{2,1,0:T(8,128)(2,1)} %bitcast.398), calls=%async_computation | async-start | bytes 3145728 | tf_op jit(solution)/shard_map/all_to_all | solution.py:168
  22.7 0.6 iota_multiply_fusion
  23.3 0.7 broadcast_convert_fusion
  24.0 0.6 slice_reduce_fusion.1
  24.8 0.5 convert_bitcast_fusion.14
  25.3 35.7 %all-to-all-done = bf16[32,24,1024]{2,1,0:T(8,128)(2,1)S(1)} async-done(((bf16[32,24,1024]{2,1,0:T(8,128)(2,1)}), bf16[32,24,1024]{2,1,0:T(8,128)(2,1)S(1)}, u32[]{:S(2)}, u32[]{:S(2)}) %all-to-all-start) | async-done | bytes 1572896 | tf_op jit(solution)/shard_map/all_to_all | solution.py:168
  61.0 1.9 collective-permute-start
  63.0 2.3 %broadcast_select_fusion.4 = (bf16[8,1,128,256]{3,2,1,0:T(8,128)(2,1)S(1)}, bf16[8,1,128,256]{3,2,1,0:T(8,128)(2,1)}) fusion(pred[]{:T(512)S(6)} %eq.83, bf16[8,2,128,128]{3,2,1,0:T(8,128)(2,1)S(1)} %bitcast.391, bf16[8,2,128,128]{3,2,1,0:T(8,128)(2,1)} %bitcast.392), kind=kLoop, calls=%fused_computation.95 | loop fusion | flops 3670016 | bytes 2097153 | tf_op jit(solution)/shard_map/jit(_where)/select_n | solution.py:200
  65.2 0.6 slice_bitcast_fusion.13
  65.9 0.7 convert_bitcast_fusion.12
  67.0 1.0 fusion.23
  68.2 2.0 fusion.45
  70.3 0.9 select_convert_fusion
  71.5 0.3 copy-done.35
  71.8 0.4 fusion.11
  72.2 1.3 convolution_convert_fusion.2
  73.5 2.3 %collective-permute-start.1 = (bf16[384,1024]{1,0:T(8,128)(2,1)}, bf16[384,1024]{1,0:T(8,128)(2,1)}, u32[]{:S(2)}, u32[]{:S(2)}) collective-permute-start(bf16[384,1024]{1,0:T(8,128)(2,1)} %convolution_convert_fusion.2), channel_id=1, source_target_pairs={{0,1},{1,0},{2,3},{3,2},{4,5},{5,4},{6,7},{7,6},{8,9},{9,8},{10,11... | collective-permute-start | bytes 2359304 | tf_op jit(solution)/shard_map/ppermute | solution.py:207
  75.8 1.5 while.29
  75.9 0.6 bitcast_dynamic-update-slice_fusion.4
  76.6 0.6 bitcast_dynamic-update-slice_fusion.4
  77.4 0.6 collective-permute-done.1
  78.0 1.5 fusion.31
  79.6 1.1 copy.138
  80.7 7.1 %all-to-all-start.1 = ((bf16[8,384,128]{2,1,0:T(8,128)(2,1)}), bf16[8,384,128]{2,1,0:T(8,128)(2,1)S(1)}, u32[]{:S(2)}, u32[]{:S(2)}) async-start(bf16[8,384,128]{2,1,0:T(8,128)(2,1)} %bitcast.389), calls=%async_computation.1 | async-start | bytes 1572864 | tf_op jit(solution)/shard_map/all_to_all | solution.py:210
  87.9 4.4 %fusion.4 = (bf16[2,64,64]{2,1,0:T(8,128)(2,1)}, f32[2,64,128,64]{2,3,1,0:T(8,128)}) fusion(f32[2,128,64]{1,2,0:T(8,128)S(1)} %copy-done.21, f32[2,128,64]{1,2,0:T(8,128)S(1)} %bitcast.399, f32[2,64,128]{2,1,0:T(8,128)S(1)} %bitcast.386, pred[64,64]{1,0:T(8,128)(4,1)S(1)} %iota_compare_fusion.10), kind=kLoop, calls=%fused_computation.11 | loop fusion | flops 5234688 | bytes 4411392 | tf_op jit(solution)/shard_map/vmap(ntd,nsd,ntsd->nts)/dot_general | solution.py:91
  92.3 1.0 convolution_convert_fusion.1
  93.3 1.0 fusion.147
  94.3 2.8 %convolution_convert_fusion.3 = bf16[256,1024]{1,0:T(8,128)(2,1)} fusion(bf16[768,1024]{1,0:T(8,128)(2,1)} %collective-permute-done, bf16[768,1024]{1,0:T(8,128)(2,1)S(1)} %bitcast.383, pred[]{:T(512)S(6)} %eq.83, bf16[767,128]{1,0:T(8,128)(2,1)S(1)} %bitcast.410, bf16[1,128]{1,0:T(2,128)(2,1)S(1)} %slice.339, bf16[768,128]{1,0:T(8,128)(2,1)S(1)} %copy-done.22), kind=kOutput, calls=%fused_computation.30 | convolution fusion | flops 404881408 | bytes 4063233 | tf_op jit(solution)/shard_map/dot_general | solution.py:225
  97.1 14.4 %all-to-all-done.1 = bf16[8,384,128]{2,1,0:T(8,128)(2,1)S(1)} async-done(((bf16[8,384,128]{2,1,0:T(8,128)(2,1)}), bf16[8,384,128]{2,1,0:T(8,128)(2,1)S(1)}, u32[]{:S(2)}, u32[]{:S(2)}) %all-to-all-start.1) | async-done | bytes 786464 | tf_op jit(solution)/shard_map/all_to_all | solution.py:210
  111.6 0.7 reshape.965
  112.3 6.5 %all-to-all-start.2 = ((bf16[32,12,128]{2,1,0:T(8,128)(2,1)}), bf16[32,12,128]{2,1,0:T(8,128)(2,1)S(1)}, u32[]{:S(2)}, u32[]{:S(2)}) async-start(bf16[32,12,128]{2,1,0:T(8,128)(2,1)} %reshape.965), calls=%async_computation.2 | async-start | bytes 262144 | tf_op jit(solution)/shard_map/all_to_all | solution.py:231
  118.8 1.9 maximum_bitcast_fusion
  120.7 7.1 %all-to-all-done.2 = bf16[32,12,128]{2,1,0:T(8,128)(2,1)S(1)} async-done(((bf16[32,12,128]{2,1,0:T(8,128)(2,1)}), bf16[32,12,128]{2,1,0:T(8,128)(2,1)S(1)}, u32[]{:S(2)}, u32[]{:S(2)}) %all-to-all-start.2) | async-done | bytes 98336 | tf_op jit(solution)/shard_map/all_to_all | solution.py:231
  127.8 1.2 broadcast_in_dim.169
  129.0 5.6 %all-to-all-start.4 = ((bf16[32,64,256]{2,1,0:T(8,128)(2,1)}), bf16[32,64,256]{2,1,0:T(8,128)(2,1)S(1)}, u32[]{:S(2)}, u32[]{:S(2)}) async-start(bf16[32,64,256]{2,1,0:T(8,128)(2,1)} %broadcast_in_dim.169), calls=%async_computation.4 | async-start | bytes 2097152 | tf_op jit(solution)/shard_map/all_to_all | solution.py:34
  134.6 0.8 maximum_bitcast_fusion.1
  135.5 0.8 maximum_bitcast_fusion.2
  136.7 16.1 %all-gather = bf16[2048,128]{1,0:T(8,128)(2,1)S(1)} all-gather(bf16[128,128]{1,0:T(8,128)(2,1)S(1)} %convolution_convert_fusion.5), channel_id=2, replica_groups=mesh['z'=8,'x'=4,'y'=8,'c'=2] {'y','c'}, dimensions={0}, use_global_device_ids=true | all-gather | bytes 557056 | tf_op jit(solution)/shard_map/all_gather | solution.py:240
  153.1 0.4 fusion.21
  153.5 8.1 %all-to-all-done.4 = bf16[32,64,256]{2,1,0:T(8,128)(2,1)S(1)} async-done(((bf16[32,64,256]{2,1,0:T(8,128)(2,1)}), bf16[32,64,256]{2,1,0:T(8,128)(2,1)S(1)}, u32[]{:S(2)}, u32[]{:S(2)}) %all-to-all-start.4) | async-done | bytes 1048608 | tf_op jit(solution)/shard_map/all_to_all | solution.py:34
  162.2 0.3 while.30
  162.8 0.7 broadcast_in_dim.173
  163.5 4.9 %all-to-all-start.5 = ((bf16[4,136,256]{2,1,0:T(8,128)(2,1)}), bf16[4,136,256]{2,1,0:T(8,128)(2,1)S(1)}, u32[]{:S(2)}, u32[]{:S(2)}) async-start(bf16[4,136,256]{2,1,0:T(8,128)(2,1)} %broadcast_in_dim.173), calls=%async_computation.5 | async-start | bytes 557056 | tf_op jit(solution)/shard_map/all_to_all | solution.py:34
  168.7 5.1 %all-to-all-done.5 = bf16[4,136,256]{2,1,0:T(8,128)(2,1)S(1)} async-done(((bf16[4,136,256]{2,1,0:T(8,128)(2,1)}), bf16[4,136,256]{2,1,0:T(8,128)(2,1)S(1)}, u32[]{:S(2)}, u32[]{:S(2)}) %all-to-all-start.5) | async-done | bytes 278560 | tf_op jit(solution)/shard_map/all_to_all | solution.py:34
  174.0 0.9 broadcast_in_dim.175
  174.8 3.5 %all-to-all-start.6 = ((bf16[8,136,256]{2,1,0:T(8,128)(2,1)}), bf16[8,136,256]{2,1,0:T(8,128)(2,1)S(1)}, u32[]{:S(2)}, u32[]{:S(2)}) async-start(bf16[8,136,256]{2,1,0:T(8,128)(2,1)} %broadcast_in_dim.175), calls=%async_computation.6 | async-start | bytes 1114112 | tf_op jit(solution)/shard_map/all_to_all | solution.py:34
  178.4 5.0 %fusion.5 = f32[2,64,128]{2,1,0:T(8,128)S(1)} fusion(f32[2,64,128,64]{2,3,1,0:T(8,128)} %get-tuple-element.289, f32[2,64,128]{2,1,0:T(8,128)S(1)} %copy-done.20, f32[2,64,64]{2,1,0:T(8,128)S(1)} %copy.105), kind=kLoop, calls=%fused_computation.13 | loop fusion | flops 3129344 | bytes 4358144 | tf_op jit(solution)/shard_map/vmap(nts,nsd,ntsd->ntd)/dot_general | solution.py:94
  183.6 1.4 convolution_convert_fusion
  185.0 2.0 multiply_reduce_fusion
  187.0 6.0 %all-to-all-done.6 = bf16[8,136,256]{2,1,0:T(8,128)(2,1)S(1)} async-done(((bf16[8,136,256]{2,1,0:T(8,128)(2,1)}), bf16[8,136,256]{2,1,0:T(8,128)(2,1)S(1)}, u32[]{:S(2)}, u32[]{:S(2)}) %all-to-all-start.6) | async-done | bytes 557088 | tf_op jit(solution)/shard_map/all_to_all | solution.py:34
  193.0 5.0 %all-to-all-start.3 = ((bf16[32,64,256]{2,1,0:T(8,128)(2,1)}), bf16[32,64,256]{2,1,0:T(8,128)(2,1)S(1)}, u32[]{:S(2)}, u32[]{:S(2)}) async-start(bf16[32,64,256]{2,1,0:T(8,128)(2,1)} %bitcast.30), calls=%async_computation.3 | async-start | bytes 2097152 | tf_op jit(solution)/shard_map/all_to_all | solution.py:260
  198.4 0.9 multiply_subtract_fusion
  199.5 0.3 fusion.81
  199.8 0.6 add_bitcast_fusion
  200.7 0.8 fusion.12
  201.6 20.1 %all-to-all-done.3 = bf16[32,64,256]{2,1,0:T(8,128)(2,1)S(1)} async-done(((bf16[32,64,256]{2,1,0:T(8,128)(2,1)}), bf16[32,64,256]{2,1,0:T(8,128)(2,1)S(1)}, u32[]{:S(2)}, u32[]{:S(2)}) %all-to-all-start.3) | async-done | bytes 1048608 | tf_op jit(solution)/shard_map/all_to_all | solution.py:260
  221.6 0.8 convert_reduce_fusion
  (157 shorter events, 6.1 us)
Async XLA Ops:
  0.6 182.9 %copy-start = (bf16[128,256]{1,0:T(8,128)(2,1)S(1)}, bf16[128,256]{1,0:T(8,128)(2,1)}, u32[]{:S(2)}) copy-start(bf16[128,256]{1,0:T(8,128)(2,1)} %param.28) | copy-start | bytes 196612
  0.6 5.5 %copy-start.2 = (bf16[128,2048]{1,0:T(8,128)(2,1)S(1)}, bf16[128,2048]{1,0:T(8,128)(2,1)}, u32[]{:S(2)}) copy-start(bf16[128,2048]{1,0:T(8,128)(2,1)} %param.19) | copy-start | bytes 1572868
  0.7 5.5 %copy-start.6 = (bf16[128,2048]{1,0:T(8,128)(2,1)S(1)}, bf16[128,2048]{1,0:T(8,128)(2,1)}, u32[]{:S(2)}) copy-start(bf16[128,2048]{1,0:T(8,128)(2,1)} %param.21) | copy-start | bytes 1572868
  5.7 0.5 copy-start.33
  9.0 13.6 %copy-start.31 = (f32[128,128]{1,0:T(8,128)S(1)}, f32[128,128]{1,0:T(8,128)}, u32[]{:S(2)}) copy-start(f32[128,128]{1,0:T(8,128)} %param.32) | copy-start | bytes 196612
  9.0 15.6 %copy-start.13 = (bf16[128,256]{1,0:T(8,128)(2,1)S(1)}, bf16[128,256]{1,0:T(8,128)(2,1)}, u32[]{:S(2)}) copy-start(bf16[128,256]{1,0:T(8,128)(2,1)} %param.31) | copy-start | bytes 196612
  9.0 15.6 %copy-start.18 = (bf16[128,128]{1,0:T(8,128)(2,1)S(1)}, bf16[128,128]{1,0:T(8,128)(2,1)}, u32[]{:S(2)}) copy-start(bf16[128,128]{1,0:T(8,128)(2,1)} %param.30) | copy-start | bytes 98308
  9.0 54.0 %copy-start.3 = (bf16[1,2048,128]{2,1,0:T(8,128)(2,1)S(1)}, bf16[1,2048,128]{2,1,0:T(8,128)(2,1)}, u32[]{:S(2)}) copy-start(bf16[1,2048,128]{2,1,0:T(8,128)(2,1)} %param.25) | copy-start | bytes 1572868
  9.0 52.0 %all-to-all-start = ((bf16[32,24,1024]{2,1,0:T(8,128)(2,1)}), bf16[32,24,1024]{2,1,0:T(8,128)(2,1)S(1)}, u32[]{:S(2)}, u32[]{:S(2)}) async-start(bf16[32,24,1024]{2,1,0:T(8,128)(2,1)} %bitcast.398), calls=%async_computation | async-start | bytes 3145728 | tf_op jit(solution)/shard_map/all_to_all | solution.py:168
  22.6 43.2 %copy-start.28 = (bf16[128,128]{1,0:T(8,128)(2,1)S(1)}, bf16[128,128]{1,0:T(8,128)(2,1)}, u32[]{:S(2)}) copy-start(bf16[128,128]{1,0:T(8,128)(2,1)} %param.29) | copy-start | bytes 98308
  61.0 5.7 %collective-permute-start = (bf16[768,1024]{1,0:T(8,128)(2,1)S(1)}, bf16[768,1024]{1,0:T(8,128)(2,1)}, u32[]{:S(2)}, u32[]{:S(2)}) collective-permute-start(bf16[768,1024]{1,0:T(8,128)(2,1)S(1)} %bitcast.381), channel_id=1, source_target_pairs={{0,1},{1,0},{2,3},{3,2},{4,5},{5,4},{6,7},{7,6},{8,9},{9,8},{10,11... | collective-permute-start | bytes 4718600 | tf_op jit(solution)/shard_map/ppermute | solution.py:169
  62.9 3.6 %copy-start.16 = (bf16[1,128,2048]{2,1,0:T(8,128)(2,1)S(1)}, bf16[1,128,2048]{2,1,0:T(8,128)(2,1)}, u32[]{:S(2)}) copy-start(bf16[1,128,2048]{2,1,0:T(8,128)(2,1)} %param.26) | copy-start | bytes 1572868
  63.0 3.6 %copy-start.4 = (bf16[1,2048,128]{2,1,0:T(8,128)(2,1)S(1)}, bf16[1,2048,128]{2,1,0:T(8,128)(2,1)}, u32[]{:S(2)}) copy-start(bf16[1,2048,128]{2,1,0:T(8,128)(2,1)} %param.24) | copy-start | bytes 1572868
  65.9 21.9 %copy-start.11 = (f32[128,128]{1,0:T(8,128)}, f32[128,128]{1,0:T(8,128)S(1)}, u32[]{:S(2)}) copy-start(f32[128,128]{1,0:T(8,128)S(1)} %convert_multiply_fusion.17) | copy-start | bytes 196612
  67.0 1.1 copy-start.8
  71.1 0.7 copy-start.35
  71.4 4.4 %copy-start.23 = (bf16[768,128]{1,0:T(8,128)(2,1)}, bf16[768,128]{1,0:T(8,128)(2,1)S(1)}, u32[]{:S(2)}) copy-start(bf16[768,128]{1,0:T(8,128)(2,1)S(1)} %get-tuple-element.266) | copy-start | bytes 589828
  71.4 4.4 %copy-start.25 = (bf16[768,128]{1,0:T(8,128)(2,1)}, bf16[768,128]{1,0:T(8,128)(2,1)S(1)}, u32[]{:S(2)}) copy-start(bf16[768,128]{1,0:T(8,128)(2,1)S(1)} %get-tuple-element.267) | copy-start | bytes 589828
  71.4 4.4 %copy-start.1 = (f32[1,1,128,256]{3,2,1,0:T(8,128)S(1)}, f32[1,1,128,256]{3,2,1,0:T(8,128)}, u32[]{:S(2)}) copy-start(f32[1,1,128,256]{3,2,1,0:T(8,128)} %param.33) | copy-start | bytes 393220
  71.5 4.4 %copy-start.36 = (f32[2,1,128]{2,1,0:T(1,128)S(1)}, f32[2,1,128]{2,1,0:T(1,128)}, u32[]{:S(2)}) copy-start(f32[2,1,128]{2,1,0:T(1,128)} %get-tuple-element.408) | copy-start | bytes 3076
  73.5 4.5 %collective-permute-start.1 = (bf16[384,1024]{1,0:T(8,128)(2,1)}, bf16[384,1024]{1,0:T(8,128)(2,1)}, u32[]{:S(2)}, u32[]{:S(2)}) collective-permute-start(bf16[384,1024]{1,0:T(8,128)(2,1)} %convolution_convert_fusion.2), channel_id=1, source_target_pairs={{0,1},{1,0},{2,3},{3,2},{4,5},{5,4},{6,7},{7,6},{8,9},{9,8},{10,11... | collective-permute-start | bytes 2359304 | tf_op jit(solution)/shard_map/ppermute | solution.py:207
  75.8 2.2 copy-start.5
  79.6 8.2 %copy-start.21 = (f32[2,128,64]{1,2,0:T(8,128)S(1)}, f32[2,128,64]{1,2,0:T(8,128)}, u32[]{:S(2)}) copy-start(f32[2,128,64]{1,2,0:T(8,128)} %get-tuple-element.296) | copy-start | bytes 196612
  80.7 30.8 %all-to-all-start.1 = ((bf16[8,384,128]{2,1,0:T(8,128)(2,1)}), bf16[8,384,128]{2,1,0:T(8,128)(2,1)S(1)}, u32[]{:S(2)}, u32[]{:S(2)}) async-start(bf16[8,384,128]{2,1,0:T(8,128)(2,1)} %bitcast.389), calls=%async_computation.1 | async-start | bytes 1572864 | tf_op jit(solution)/shard_map/all_to_all | solution.py:210
  87.8 4.4 %copy-start.26 = (bf16[768,128]{1,0:T(8,128)(2,1)S(1)}, bf16[768,128]{1,0:T(8,128)(2,1)}, u32[]{:S(2)}) copy-start(bf16[768,128]{1,0:T(8,128)(2,1)} %copy-done.25) | copy-start | bytes 589828
  87.8 4.4 %copy-start.24 = (bf16[768,128]{1,0:T(8,128)(2,1)S(1)}, bf16[768,128]{1,0:T(8,128)(2,1)}, u32[]{:S(2)}) copy-start(bf16[768,128]{1,0:T(8,128)(2,1)} %copy-done.23) | copy-start | bytes 589828
  87.8 4.4 %copy-start.22 = (bf16[768,128]{1,0:T(8,128)(2,1)S(1)}, bf16[768,128]{1,0:T(8,128)(2,1)}, u32[]{:S(2)}) copy-start(bf16[768,128]{1,0:T(8,128)(2,1)} %get-tuple-element.264) | copy-start | bytes 589828
  87.8 4.4 %copy-start.9 = (bf16[768,1024]{1,0:T(8,128)(2,1)S(1)}, bf16[768,1024]{1,0:T(8,128)(2,1)}, u32[]{:S(2)}) copy-start(bf16[768,1024]{1,0:T(8,128)(2,1)} %copy-done.8) | copy-start | bytes 4718596
  97.1 30.7 %copy-start.32 = (bf16[64,256]{1,0:T(8,128)(2,1)S(1)}, bf16[64,256]{1,0:T(8,128)(2,1)}, u32[]{:S(2)}) copy-start(bf16[64,256]{1,0:T(8,128)(2,1)} %param.27) | copy-start | bytes 98308
  112.3 15.5 %all-to-all-start.2 = ((bf16[32,12,128]{2,1,0:T(8,128)(2,1)}), bf16[32,12,128]{2,1,0:T(8,128)(2,1)S(1)}, u32[]{:S(2)}, u32[]{:S(2)}) async-start(bf16[32,12,128]{2,1,0:T(8,128)(2,1)} %reshape.965), calls=%async_computation.2 | async-start | bytes 262144 | tf_op jit(solution)/shard_map/all_to_all | solution.py:231
  120.7 13.9 %copy-start.10 = (bf16[1024,128]{1,0:T(8,128)(2,1)S(1)}, bf16[1024,128]{1,0:T(8,128)(2,1)}, u32[]{:S(2)}) copy-start(bf16[1024,128]{1,0:T(8,128)(2,1)} %get-tuple-element.275) | copy-start | bytes 786436
  129.0 6.5 %copy-start.17 = (bf16[256,1024]{1,0:T(8,128)(2,1)S(1)}, bf16[256,1024]{1,0:T(8,128)(2,1)}, u32[]{:S(2)}) copy-start(bf16[256,1024]{1,0:T(8,128)(2,1)} %convolution_convert_fusion.3) | copy-start | bytes 1572868
  129.0 32.6 %all-to-all-start.4 = ((bf16[32,64,256]{2,1,0:T(8,128)(2,1)}), bf16[32,64,256]{2,1,0:T(8,128)(2,1)S(1)}, u32[]{:S(2)}, u32[]{:S(2)}) async-start(bf16[32,64,256]{2,1,0:T(8,128)(2,1)} %broadcast_in_dim.169), calls=%async_computation.4 | async-start | bytes 2097152 | tf_op jit(solution)/shard_map/all_to_all | solution.py:34
  134.6 1.8 copy-start.39
  134.6 1.8 copy-start.40
  135.5 17.3 %copy-start.30 = (f32[2048]{0:T(1024)S(1)}, f32[2048]{0:T(1024)}, u32[]{:S(2)}) copy-start(f32[2048]{0:T(1024)} %param.20) | copy-start | bytes 24580
  135.5 17.3 %copy-start.34 = (f32[128]{0:T(128)S(1)}, f32[128]{0:T(128)}, u32[]{:S(2)}) copy-start(f32[128]{0:T(128)} %copy-done.33) | copy-start | bytes 1540
  135.5 17.6 %copy-start.7 = (bf16[128,2048]{1,0:T(8,128)(2,1)S(1)}, bf16[128,2048]{1,0:T(8,128)(2,1)}, u32[]{:S(2)}) copy-start(bf16[128,2048]{1,0:T(8,128)(2,1)} %param.21) | copy-start | bytes 1572868
  153.1 8.8 %copy-start.12 = (f32[128,128]{1,0:T(8,128)S(1)}, f32[128,128]{1,0:T(8,128)}, u32[]{:S(2)}) copy-start(f32[128,128]{1,0:T(8,128)} %copy-done.11) | copy-start | bytes 196612
  153.5 8.7 %copy-start.37 = (f32[2,1,128]{2,1,0:T(1,128)S(1)}, f32[2,1,128]{2,1,0:T(1,128)}, u32[]{:S(2)}) copy-start(f32[2,1,128]{2,1,0:T(1,128)} %get-tuple-element.408) | copy-start | bytes 3076
  162.2 0.6 copy-start.38
  162.2 6.3 %copy-start.14 = (bf16[128,256]{1,0:T(8,128)(2,1)S(1)}, bf16[128,256]{1,0:T(8,128)(2,1)}, u32[]{:S(2)}) copy-start(bf16[128,256]{1,0:T(8,128)(2,1)} %param.31) | copy-start | bytes 196612
  163.5 14.8 %copy-start.20 = (f32[2,64,128]{2,1,0:T(8,128)S(1)}, f32[2,64,128]{2,1,0:T(8,128)}, u32[]{:S(2)}) copy-start(f32[2,64,128]{2,1,0:T(8,128)} %get-tuple-element.297) | copy-start | bytes 196612
  163.5 10.2 %all-to-all-start.5 = ((bf16[4,136,256]{2,1,0:T(8,128)(2,1)}), bf16[4,136,256]{2,1,0:T(8,128)(2,1)S(1)}, u32[]{:S(2)}, u32[]{:S(2)}) async-start(bf16[4,136,256]{2,1,0:T(8,128)(2,1)} %broadcast_in_dim.173), calls=%async_computation.5 | async-start | bytes 557056 | tf_op jit(solution)/shard_map/all_to_all | solution.py:34
  174.8 18.2 %all-to-all-start.6 = ((bf16[8,136,256]{2,1,0:T(8,128)(2,1)}), bf16[8,136,256]{2,1,0:T(8,128)(2,1)S(1)}, u32[]{:S(2)}, u32[]{:S(2)}) async-start(bf16[8,136,256]{2,1,0:T(8,128)(2,1)} %broadcast_in_dim.175), calls=%async_computation.6 | async-start | bytes 1114112 | tf_op jit(solution)/shard_map/all_to_all | solution.py:34
  178.4 5.0 %copy-start.15 = (bf16[2,1,128,256]{3,2,1,0:T(8,128)(2,1)S(1)}, bf16[2,1,128,256]{3,2,1,0:T(8,128)(2,1)}, u32[]{:S(2)}) copy-start(bf16[2,1,128,256]{3,2,1,0:T(8,128)(2,1)} %get-tuple-element.142) | copy-start | bytes 393220
  187.0 11.4 %copy-start.19 = (bf16[128,128]{1,0:T(8,128)(2,1)S(1)}, bf16[128,128]{1,0:T(8,128)(2,1)}, u32[]{:S(2)}) copy-start(bf16[128,128]{1,0:T(8,128)(2,1)} %param.30) | copy-start | bytes 98308
  187.0 11.4 %copy-start.29 = (bf16[128,128]{1,0:T(8,128)(2,1)S(1)}, bf16[128,128]{1,0:T(8,128)(2,1)}, u32[]{:S(2)}) copy-start(bf16[128,128]{1,0:T(8,128)(2,1)} %param.29) | copy-start | bytes 98308
  193.0 28.6 %all-to-all-start.3 = ((bf16[32,64,256]{2,1,0:T(8,128)(2,1)}), bf16[32,64,256]{2,1,0:T(8,128)(2,1)S(1)}, u32[]{:S(2)}, u32[]{:S(2)}) async-start(bf16[32,64,256]{2,1,0:T(8,128)(2,1)} %bitcast.30), calls=%async_computation.3 | async-start | bytes 2097152 | tf_op jit(solution)/shard_map/all_to_all | solution.py:260
  198.4 2.3 %copy-start.27 = (bf16[2,64,64]{2,1,0:T(8,128)(2,1)S(1)}, bf16[2,64,64]{2,1,0:T(8,128)(2,1)}, u32[]{:S(2)}) copy-start(bf16[2,64,64]{2,1,0:T(8,128)(2,1)} %get-tuple-element.288) | copy-start | bytes 49156
